TPU v7x, 32 devices: a whole 2x2x4 slice. The times are simulated.
32 devices in a mesh: sp: 4 (over z), fs: 4 (over y, x), tp: 2 (over core).
Axes of the slice: x: 2, y: 2, z: 4, core: 2. Of those that a mesh axis runs over, the one named last changes fastest.
Arguments:
- stream: bfloat16 [4, 4096, 2048], P('fs', 'sp', 'tp'), parts along dimension 0, may hold values from -6 to 6
- w_pool_in: bfloat16 [2048, 1024], P(None, 'tp'), may hold values from -0.125 to 0.125
- w_query: bfloat16 [2048, 1024], P(None, 'tp'), may hold values from -0.125 to 0.125
- w_forget: bfloat16 [2048, 1024], P(None, 'tp'), may hold values from -0.125 to 0.125
- w_value: bfloat16 [2048, 1024], P(None, 'tp'), may hold values from -0.125 to 0.125
- w_outgate: bfloat16 [2048, 1024], P(None, 'tp'), may hold values from -0.125 to 0.125
- pool_mix: bfloat16 [4, 256, 256], P('tp'), may hold values from -0.375 to 0.375
- pool_scale: float32 [1024], P('tp'), may hold values from 0.1 to 1.9
- lower_bound: float32 [1024], P('tp'), may hold values from 0.9 to 1
- extra_decay: float32 [4096, 8], P('sp', 'tp'), may hold values from -0.7 to 0
- rec_gain: float32 [128], replicated, may hold values from 0.1 to 1.9
- w_out_pool: bfloat16 [1024, 2048], P('tp'), may hold values from -0.125 to 0.125
- w_out_rec: bfloat16 [1024, 2048], P('tp'), may hold values from -0.125 to 0.125
- norm_gain: float32 [2048], P('tp'), may hold values from 0.1 to 1.9
- norm_bias: float32 [2048], P('tp'), may hold values from -3 to 3
Outputs:
- layer_out: bfloat16 [4, 4096, 2048], P('fs', 'sp', 'tp'), parts along dimension 0
There are 4 independent parts, one for each index of `fs`. A program takes and returns all parts, laid end to end along the dimension named above; an argument that names none is the same for every part. Nothing has to cross between parts.
All inputs are finite; a program needn't handle non-finite values.
Results may differ from a plain program's by a relative error of at most 0.0085.
Values may be sent and summed in bfloat16 or wider, within the bound.
A program may use at most 128 MiB of HBM per device.

v0:
```python
import functools

import jax
import jax.numpy as jnp
from jax import lax
from jax.experimental import pallas as pl
from jax.experimental.pallas import tpu as pltpu
from jax.sharding import PartitionSpec as P

DK = 128
BLOCK_ROWS = 128
GROUP_CH = 256
HALO = 16
LANES = 128

ALPHA = 2.0**0.25
EPS_RMS = 1e-06
EPS_NORM = 1e-05
F32 = jnp.float32
BF16 = jnp.bfloat16
NT = (((1,), (1,)), ((), ()))
TN = (((0,), (0,)), ((), ()))


def dot(a, b, dims=None):
    if dims is None:
        return jnp.dot(a, b, preferred_element_type=F32)
    return lax.dot_general(a, b, dims, preferred_element_type=F32)


def half_sigmoid(x):
    return 0.5 + 0.5 * jnp.tanh(0.5 * x)


def mixer(
    n_sp, n_tp, rows_x,
    stream, w_pool, w_query, w_forget, w_value, w_gate,
    mix_in, scale_in, bound_in, extra_in, gain_in, wo_pool, wo_rec,
    out, stats,
    x_buf, w_buf, wo_buf, a_buf, v_buf, u_buf, e_buf, t_buf, p_buf, q_buf, g_buf, r_buf,
    o_buf, half_buf, state, state_out, state_in, halo_in, stat_own, stat_peer, stat_sum,
    mix, scale, bound, extra, gain,
    x_loc, x_send, x_recv, w_sem, wo_loc, wo_send, wo_recv, a_send, a_recv,
    st_send, st_recv, h_send, h_recv, s_send, s_recv, o_sem, t_sem, small_sem,
):
    sp, tp = lax.axis_index("sp"), lax.axis_index("tp")
    peer = 1 - tp
    length, feats = stream.shape[1], stream.shape[2]
    chans = bound.shape[1]
    heads = chans // DK
    pool_w = scale.shape[1]
    groups = mix.shape[0]
    chunks = length // rows_x
    blocks = length // BLOCK_ROWS
    per = rows_x // BLOCK_ROWS
    wide_x = 2 * rows_x
    wides, wide_per = length // wide_x, wide_x // BLOCK_ROWS

    def x_in(c):
        rows = pl.ds(c * rows_x, rows_x)
        return pltpu.make_async_copy(stream.at[0, rows], x_buf.at[tp, rows], x_loc.at[c])

    def x_out(c):
        rows = pl.ds(c * rows_x, rows_x)
        return pltpu.make_async_remote_copy(
            x_buf.at[tp, rows], x_buf.at[tp, rows], x_send.at[c], x_recv.at[c],
            device_id={"tp": peer}, device_id_type=pl.DeviceIdType.MESH)

    def w_in(i):
        src = (w_forget, w_value, w_pool, w_query, w_gate)[i]
        return [
            pltpu.make_async_copy(src.at[pl.ds(k * feats, feats)], w_buf.at[i, k], w_sem.at[i, k])
            for k in range(n_tp)
        ]

    my_cols = pl.ds(pl.multiple_of(tp * feats, LANES), feats)
    peer_cols = pl.ds(pl.multiple_of(peer * feats, LANES), feats)
    wo_places = ((wo_pool, pl.ds(0, pool_w)), (wo_rec, pl.ds(pool_w, chans)))

    def wo_in(i):
        src, place = wo_places[i]
        return pltpu.make_async_copy(src.at[:, my_cols], wo_buf.at[tp, place], wo_loc.at[i])

    def wo_out(i):
        src, place = wo_places[i]
        return pltpu.make_async_remote_copy(
            src.at[:, peer_cols], wo_buf.at[tp, place], wo_send.at[i], wo_recv.at[i],
            device_id={"tp": peer}, device_id_type=pl.DeviceIdType.MESH)

    def a_out(i, c):
        rows, cols = pl.ds(c * rows_x, rows_x), wo_places[i][1]
        return pltpu.make_async_remote_copy(
            a_buf.at[tp, rows, cols], a_buf.at[tp, rows, cols], a_send.at[i, c], a_recv.at[i, c],
            device_id={"tp": peer}, device_id_type=pl.DeviceIdType.MESH)

    def st_out(k, slot):
        return pltpu.make_async_remote_copy(
            state_out, state_in.at[slot], st_send.at[k], st_recv.at[slot],
            device_id={"sp": k}, device_id_type=pl.DeviceIdType.MESH)

    def h_out(k):
        return pltpu.make_async_remote_copy(
            p_buf.at[pl.ds(BLOCK_ROWS + length - HALO, HALO)], halo_in, h_send, h_recv,
            device_id={"sp": k}, device_id_type=pl.DeviceIdType.MESH)

    def s_out(c):
        return pltpu.make_async_remote_copy(
            stat_own.at[c], stat_peer.at[c], s_send.at[c], s_recv.at[c],
            device_id={"tp": peer}, device_id_type=pl.DeviceIdType.MESH)

    def o_out(c):
        rows = pl.ds(c * rows_x, rows_x)
        return pltpu.make_async_copy(o_buf.at[rows], out.at[rows], o_sem.at[c])

    def t_out(c):
        rows = pl.ds(c * rows_x, rows_x)
        return pltpu.make_async_copy(stat_sum.at[c], stats.at[rows], t_sem.at[c])

    smalls = [
        pltpu.make_async_copy(src, dst, small_sem.at[i])
        for i, (src, dst) in enumerate(
            ((bound_in, bound), (extra_in, extra), (mix_in, mix), (scale_in, scale), (gain_in, gain)))
    ]

    for c in range(chunks):
        x_in(c).start()
        if c == 0:
            for i in (0, 1):
                for copy in w_in(i):
                    copy.start()
            for copy in smalls:
                copy.start()

    barrier = pltpu.get_barrier_semaphore()
    pl.semaphore_signal(barrier, inc=1, device_id={"tp": peer}, device_id_type=pl.DeviceIdType.MESH)
    for step in range(1, n_sp):
        pl.semaphore_signal(
            barrier, inc=1, device_id={"sp": lax.rem(sp + step, n_sp)},
            device_id_type=pl.DeviceIdType.MESH)
    p_buf[pl.ds(0, BLOCK_ROWS), :] = jnp.zeros((BLOCK_ROWS, pool_w), BF16)
    state[...] = jnp.zeros_like(state)
    pl.semaphore_wait(barrier, n_sp)

    for c in range(chunks):
        x_in(c).wait()
        x_out(c).start()

    row_ids = lax.broadcasted_iota(jnp.int32, (BLOCK_ROWS, BLOCK_ROWS), 0)
    col_ids = lax.broadcasted_iota(jnp.int32, (BLOCK_ROWS, BLOCK_ROWS), 1)
    lower = row_ids >= col_ids
    tri = jnp.where(lower, 1.0, 0.0).astype(BF16)
    lower_twice = jnp.concatenate([row_ids, row_ids], axis=1) >= jnp.concatenate([col_ids, col_ids], axis=1)
    tri_twice = jnp.concatenate([tri, tri], axis=1)
    ones = jnp.ones((2 * BLOCK_ROWS, DK), BF16)

    for i in (0, 1):
        for copy in w_in(i):
            copy.wait()
    for copy in smalls:
        copy.wait()
    for i in (2, 3, 4):
        for copy in w_in(i):
            copy.start()
    for i in range(2):
        wo_in(i).start()
        wo_out(i).start()

    def first(c, _):
        rows = pl.ds(pl.multiple_of(c * wide_x, wide_x), wide_x)
        own = x_buf[tp, rows]
        f_own = dot(own, w_buf[0, tp])
        v_own = dot(own, w_buf[1, tp])
        for k in range(2):
            x_out(2 * c + k).wait_recv()
        other = x_buf[peer, rows]
        f_in = (f_own + dot(other, w_buf[0, peer])).astype(BF16).astype(F32)
        vals = (v_own + dot(other, w_buf[1, peer])).astype(BF16)
        v_buf[rows, :] = vals
        open_part = 1.0 - bound[...]
        for j in range(wide_per):
            part = slice(j * BLOCK_ROWS, (j + 1) * BLOCK_ROWS)
            b = c * wide_per + j
            brows = pl.ds(pl.multiple_of(b * BLOCK_ROWS, BLOCK_ROWS), BLOCK_ROWS)
            weight = open_part * (0.5 - 0.5 * jnp.tanh(0.5 * f_in[part]))
            keep = jnp.log(1.0 - weight)
            high = keep.astype(BF16)
            low = (keep - high.astype(F32)).astype(BF16)
            drop = extra[:, brows]
            drop_high = drop.astype(BF16).astype(F32)
            drop_low = drop - drop_high
            drops = []
            for h in range(heads):
                pair = jnp.concatenate([drop_high[h:h + 1], drop_low[h:h + 1]], axis=1)
                wide = jnp.where(lower_twice, jnp.broadcast_to(pair, (BLOCK_ROWS, 2 * BLOCK_ROWS)), 0.0)
                drops.append(dot(wide.astype(BF16), ones))
            total = dot(tri_twice, jnp.concatenate([high, low], axis=0)) + jnp.concatenate(drops, axis=1)
            middle = 0.5 * total[BLOCK_ROWS - 1:BLOCK_ROWS]
            e_buf[brows, :] = jnp.exp(total - middle)
            down = (weight * jnp.exp(middle - total)).astype(BF16)
            u_buf[brows, :] = down
            half = jnp.exp(middle)
            half_buf[b] = jnp.broadcast_to(half, (8, chans))
            for h in range(heads):
                lanes = slice(h * DK, (h + 1) * DK)
                hh = half[:, lanes]
                term = dot(vals[part, lanes], down[:, lanes], TN) * hh
                t_buf[b, :, lanes] = term
                state[:, lanes] = hh * hh * state[:, lanes] + term
        return 0

    lax.fori_loop(0, wides, first, 0)

    for copy in w_in(2):
        copy.wait()

    def second(c, _):
        start = c * rows_x if isinstance(c, int) else pl.multiple_of(c * rows_x, rows_x)
        rows = pl.ds(start, rows_x)
        pooled = dot(x_buf[tp, rows], w_buf[2, tp]) + dot(x_buf[peer, rows], w_buf[2, peer])
        p_buf[pl.ds(start + BLOCK_ROWS, rows_x), :] = pooled.astype(BF16)
        return 0

    second(chunks - 1, 0)

    @pl.when(sp + 1 < n_sp)
    def _():
        h_out(sp + 1).start()

    log_half = half_buf[0, 0:1]
    for b in range(1, blocks):
        log_half = log_half * half_buf[b, 0:1]
    state_out[pl.ds(0, DK), :] = state[...].astype(BF16)
    state_out[pl.ds(DK, HALO), :] = jnp.broadcast_to(log_half * log_half, (HALO, chans)).astype(BF16)

    def send_state(k, _):
        st_out(k, sp).start()
        return 0

    lax.fori_loop(sp + 1, n_sp, send_state, 0)

    lax.fori_loop(0, chunks - 1, second, 0)

    for i in (3, 4):
        for copy in w_in(i):
            copy.wait()

    wide_rows = lax.broadcasted_iota(jnp.int32, (BLOCK_ROWS, 2 * BLOCK_ROWS), 0) + BLOCK_ROWS
    wide_cols = lax.broadcasted_iota(jnp.int32, (BLOCK_ROWS, 2 * BLOCK_ROWS), 1)
    back = wide_rows - wide_cols
    count = lax.broadcasted_iota(jnp.int32, (BLOCK_ROWS, LANES), 0) + (sp * length + 1)

    def third(step, _):
        c = wides - 1 - step

        @pl.when((step == wides - 1) & (sp > 0))
        def _():
            h_out(sp).wait_recv()
            p_buf[pl.ds(BLOCK_ROWS - HALO, HALO), :] = halo_in[...]

        rows = pl.ds(pl.multiple_of(c * wide_x, wide_x), wide_x)
        own, other = x_buf[tp, rows], x_buf[peer, rows]
        q_in = (dot(own, w_buf[3, tp]) + dot(other, w_buf[3, peer])).astype(BF16).astype(F32)
        ups = (q_in * half_sigmoid(q_in) * e_buf[rows, :]).astype(BF16)
        q_buf[rows, :] = ups
        g_in = dot(own, w_buf[4, tp]) + dot(other, w_buf[4, peer])
        g_buf[rows, :] = g_in.astype(BF16)
        for k in range(wide_per):
            start = pl.multiple_of(c * wide_x + k * BLOCK_ROWS, BLOCK_ROWS)
            brows = pl.ds(start, BLOCK_ROWS)
            near = p_buf[pl.ds(start, 2 * BLOCK_ROWS), :]
            for j in range(groups):
                lanes = slice(j * GROUP_CH, (j + 1) * GROUP_CH)
                window = jnp.left_shift(jnp.int32(2), tp * groups + j)
                band = jnp.where((back >= 0) & (back < window), 1.0, 0.0).astype(BF16)
                share = 1.0 / jnp.minimum(count + start, window).astype(F32)
                share = jnp.concatenate([share] * (GROUP_CH // LANES), axis=1)
                sums = dot(band, near[:, lanes])
                diff = (sums * share - near[BLOCK_ROWS:, lanes].astype(F32)).astype(BF16)
                a_buf[tp, brows, lanes] = (dot(diff, mix[j]) * scale[:, lanes]).astype(BF16)
            for h in range(heads):
                lanes = slice(h * DK, (h + 1) * DK)
                up = ups[k * BLOCK_ROWS:(k + 1) * BLOCK_ROWS, lanes]
                scores = jnp.where(lower, dot(up, u_buf[brows, lanes], NT), 0.0).astype(BF16)
                e_buf[brows, lanes] = dot(scores, v_buf[brows, lanes])
        for k in range(2):
            a_out(0, 2 * c + k).start()
        return 0

    lax.fori_loop(0, wides, third, 0)

    for i in range(2):
        wo_in(i).wait()
        wo_out(i).wait_recv()

    pool_at, rec_at = wo_places[0][1], wo_places[1][1]

    def pool_part(step, _):
        c = chunks - 1 - step
        rows = pl.ds(pl.multiple_of(c * rows_x, rows_x), rows_x)
        mine = dot(a_buf[tp, rows, pool_at], wo_buf[tp, pool_at]) + ALPHA * x_buf[tp, rows].astype(F32)
        a_out(0, c).wait_recv()
        r_buf[rows, :] = mine + dot(a_buf[peer, rows, pool_at], wo_buf[peer, pool_at])
        return 0

    lax.fori_loop(0, chunks, pool_part, 0)

    state[...] = jnp.zeros_like(state)

    def join(k, _):
        st_out(sp, k).wait_recv()
        keep = state_in[k, pl.ds(DK, HALO), :].astype(F32)[0:1]
        state[...] = keep * state[...] + state_in[k, pl.ds(0, DK), :].astype(F32)
        return 0

    lax.fori_loop(0, sp, join, 0)

    def fourth(c, _):
        for k in range(per):
            b = c * per + k
            rows = pl.ds(pl.multiple_of(b * BLOCK_ROWS, BLOCK_ROWS), BLOCK_ROWS)
            half = half_buf[b, 0:1]
            before = state[...] * half
            carried = before.astype(BF16)
            state[...] = before * half + t_buf[b]
            for h in range(heads):
                lanes = slice(h * DK, (h + 1) * DK)
                raw = e_buf[rows, lanes] + dot(q_buf[rows, lanes], carried[:, lanes], NT)
                power = jnp.mean(raw * raw, axis=-1, keepdims=True)
                gate = g_buf[rows, lanes].astype(F32)
                rec = raw * lax.rsqrt(power + EPS_RMS) * gain[...] * (gate * half_sigmoid(gate))
                a_buf[tp, rows, pool_w + h * DK:pool_w + (h + 1) * DK] = rec.astype(BF16)
        a_out(1, c).start()
        return 0

    lax.fori_loop(0, chunks, fourth, 0)

    def fold(x):
        acc = x[:, :LANES]
        for k in range(1, feats // LANES):
            acc = acc + x[:, k * LANES:(k + 1) * LANES]
        return acc

    first_half = lax.broadcasted_iota(jnp.int32, (rows_x, LANES), 1) < LANES // 2

    def fifth(c, _):
        rows = pl.ds(pl.multiple_of(c * rows_x, rows_x), rows_x)
        mine = r_buf[rows, :] + dot(a_buf[tp, rows, rec_at], wo_buf[tp, rec_at])
        a_out(1, c).wait_recv()
        resid = mine + dot(a_buf[peer, rows, rec_at], wo_buf[peer, rec_at])
        o_buf[rows, :] = resid.astype(BF16)
        sums, squares = fold(resid), fold(resid * resid)
        sums = sums + pltpu.roll(sums, LANES // 2, 1)
        squares = squares + pltpu.roll(squares, LANES // 2, 1)
        stat_own[c] = jnp.where(first_half, sums, squares)
        s_out(c).start()
        o_out(c).start()
        return 0

    lax.fori_loop(0, chunks, fifth, 0)

    for c in range(chunks):
        s_out(c).wait_recv()
        stat_sum[c] = stat_own[c] + stat_peer[c]
        t_out(c).start()

    for c in range(chunks):
        x_out(c).wait_send()
        s_out(c).wait_send()
        o_out(c).wait()
        t_out(c).wait()
        for i in range(2):
            a_out(i, c).wait_send()
    for i in range(2):
        wo_out(i).wait_send()

    def sent_state(k, _):
        st_out(k, sp).wait_send()
        return 0

    lax.fori_loop(sp + 1, n_sp, sent_state, 0)

    @pl.when(sp + 1 < n_sp)
    def _():
        h_out(sp + 1).wait_send()


def finish(width, rows, resid, stats, norm_gain, norm_bias, out,
           r_buf, s_buf, o_buf, gain, bias, r_sem, s_sem, o_sem, n_sem):
    pieces = resid.shape[0] // rows

    def copies(c):
        part = pl.ds(c * rows, rows)
        return (
            pltpu.make_async_copy(stats.at[part], s_buf.at[part], s_sem.at[c]),
            pltpu.make_async_copy(resid.at[part], r_buf.at[part], r_sem.at[c]),
            pltpu.make_async_copy(o_buf.at[part], out.at[0, part], o_sem.at[c]),
        )

    norms = (
        pltpu.make_async_copy(norm_gain, gain, n_sem.at[0]),
        pltpu.make_async_copy(norm_bias, bias, n_sem.at[1]),
    )
    for copy in norms:
        copy.start()
    for c in range(pieces):
        for copy in copies(c)[:2]:
            copy.start()
    for copy in norms:
        copy.wait()
    first_half = lax.broadcasted_iota(jnp.int32, (rows, LANES), 1) < LANES // 2
    for c in range(pieces):
        part = pl.ds(c * rows, rows)
        for copy in copies(c)[:2]:
            copy.wait()
        both = s_buf[part, :]
        mean = jnp.sum(jnp.where(first_half, both, 0.0), axis=1, keepdims=True) / width
        square = jnp.sum(jnp.where(first_half, 0.0, both), axis=1, keepdims=True) / width
        inv = lax.rsqrt(square - mean * mean + EPS_NORM)
        o_buf[part, :] = ((r_buf[part, :].astype(F32) - mean) * inv * gain[...] + bias[...]).astype(BF16)
        copies(c)[2].start()
    for c in range(pieces):
        copies(c)[2].wait()


def solution(mesh):
    n_sp, n_tp = mesh.shape["sp"], mesh.shape["tp"]

    def local(stream, w_pool, w_query, w_forget, w_value, w_gate, mix, scale, bound, extra,
              gain, wo_pool, wo_rec, norm_gain, norm_bias):
        length, feats = stream.shape[1], stream.shape[2]
        chans, pool_w = bound.shape[0], scale.shape[0]
        blocks = length // BLOCK_ROWS
        rows_x = 256
        chunks = length // rows_x
        hbm = pl.BlockSpec(memory_space=pl.ANY)
        dma = pltpu.SemaphoreType.DMA
        scratch = [
            pltpu.VMEM((n_tp, length, feats), BF16),
            pltpu.VMEM((5, n_tp, feats, chans), BF16),
            pltpu.VMEM((n_tp, pool_w + chans, feats), BF16),
            pltpu.VMEM((n_tp, length, pool_w + chans), BF16),
            pltpu.VMEM((length, chans), BF16),
            pltpu.VMEM((length, chans), BF16),
            pltpu.VMEM((length, chans), F32),
            pltpu.VMEM((blocks, DK, chans), F32),
            pltpu.VMEM((BLOCK_ROWS + length, pool_w), BF16),
            pltpu.VMEM((length, chans), BF16),
            pltpu.VMEM((length, chans), BF16),
            pltpu.VMEM((length, feats), F32),
            pltpu.VMEM((length, feats), BF16),
            pltpu.VMEM((blocks, 8, chans), F32),
            pltpu.VMEM((DK, chans), F32),
            pltpu.VMEM((DK + HALO, chans), BF16),
            pltpu.VMEM((n_sp, DK + HALO, chans), BF16),
            pltpu.VMEM((HALO, pool_w), BF16),
            pltpu.VMEM((chunks, rows_x, LANES), F32),
            pltpu.VMEM((chunks, rows_x, LANES), F32),
            pltpu.VMEM((chunks, rows_x, LANES), F32),
            pltpu.VMEM(mix.shape, BF16),
            pltpu.VMEM((1, pool_w), F32),
            pltpu.VMEM((1, chans), F32),
            pltpu.VMEM((chans // DK, length), F32),
            pltpu.VMEM((1, DK), F32),
            dma((chunks,)), dma((chunks,)), dma((chunks,)), dma((5, n_tp)),
            dma((2,)), dma((2,)), dma((2,)), dma((2, chunks)), dma((2, chunks)),
            dma((n_sp,)), dma((n_sp,)), dma, dma, dma((chunks,)), dma((chunks,)), dma((chunks,)),
            dma((chunks,)), dma((5,)),
        ]
        row = lambda x: x.reshape(1, -1)
        resid, stats = pl.pallas_call(
            functools.partial(mixer, n_sp, n_tp, rows_x),
            out_shape=(
                jax.ShapeDtypeStruct((length, feats), BF16), jax.ShapeDtypeStruct((length, LANES), F32)),
            in_specs=[hbm] * 13,
            out_specs=(hbm, hbm),
            scratch_shapes=scratch,
            compiler_params=pltpu.CompilerParams(
                collective_id=0, has_side_effects=True, vmem_limit_bytes=60 * 1024 * 1024),
            name="mixer",
        )(stream, w_pool, w_query, w_forget, w_value, w_gate, mix, row(scale), row(bound), extra.T,
          row(gain), wo_pool, wo_rec)
        piece = 128
        pieces = length // piece
        return pl.pallas_call(
            functools.partial(finish, n_tp * feats, piece),
            out_shape=jax.ShapeDtypeStruct(stream.shape, BF16),
            in_specs=[hbm] * 4,
            out_specs=hbm,
            scratch_shapes=[
                pltpu.VMEM((length, feats), BF16),
                pltpu.VMEM((length, LANES), F32),
                pltpu.VMEM((length, feats), BF16),
                pltpu.VMEM((1, feats), F32),
                pltpu.VMEM((1, feats), F32),
                dma((pieces,)), dma((pieces,)), dma((pieces,)), dma((2,)),
            ],
            compiler_params=pltpu.CompilerParams(vmem_limit_bytes=60 * 1024 * 1024),
            name="finish",
        )(resid, stats, row(norm_gain), row(norm_bias))

    placed = (
        P("fs", "sp", "tp"), P(None, "tp"), P(None, "tp"), P(None, "tp"), P(None, "tp"),
        P(None, "tp"), P("tp", None, None), P("tp"), P("tp"), P("sp", "tp"), P(),
        P("tp", None), P("tp", None), P("tp"), P("tp"),
    )
    return jax.shard_map(
        local, mesh=mesh, in_specs=placed, out_specs=P("fs", "sp", "tp"), check_vma=False
    )
```

profile of v0, /device:TPU:0, one launch (start us, length us, event | category | flops | bytes accessed | tf_op | source)
XLA Modules:
  0.0 42.7 jit_solution(4598713406061029192)
XLA Ops:
  0.0 38.8 %mixer.1 = (bf16[1024,1024]{1,0:T(8,128)(2,1)}, f32[1024,128]{1,0:T(8,128)}) custom-call(bf16[1,1024,1024]{2,1,0:T(8,128)(2,1)} %stream.1, bf16[2048,512]{1,0:T(8,128)(2,1)} %w_pool.1, bf16[2048,512]{1,0:T(8,128)(2,1)} %w_query.1, bf16[2048,512]{1,0:T(8,128)(2,1)} %w_forget.1, bf16[2048,512]{1,0:T(8,128)(2,1)} %w_value.1, bf16[2048,512]{1,0:T(8,128)(2,1)} %w_gate.1, ...), custom_call_target="tpu_custom_call" | custom-call | tf_op jit(solution)/shard_map/mixer/pallas_call | solution.py:470
  38.8 3.8 %finish.1 = bf16[1,1024,1024]{2,1,0:T(8,128)(2,1)} custom-call(bf16[1024,1024]{1,0:T(8,128)(2,1)} %get-tuple-element.7.resid, f32[1024,128]{1,0:T(8,128)} %get-tuple-element.8.stats, f32[1,1024]{1,0:T(1,128)} %bitcast.7, f32[1,1024]{1,0:T(1,128)} %bitcast.8), custom_call_target="tpu_custom_call" | custom-call | tf_op jit(solution)/shard_map/finish/pallas_call | solution.py:484
where the time goes:
time: 42.8 us; the launch traced here: 42.7 us
  Pallas kernels  42.7 us (100%)
    pallas_call x1, Pallas kernels, local(): pl.pallas_call(functools.partial(mixer, n_sp, n_tp, rows_x), out_shape=(j...  38.8 us
    pallas_call x1, Pallas kernels, local(): pl.pallas_call(functools.partial(finish, n_tp * feats, piece), out_shape=...  3.84 us

commit v1 on v0

--- a/solution.py
+++ b/solution.py
@@ -41,7 +41,7 @@
     o_buf, half_buf, state, state_out, state_in, halo_in, stat_own, stat_peer, stat_sum,
     mix, scale, bound, extra, gain,
     x_loc, x_send, x_recv, w_sem, wo_loc, wo_send, wo_recv, a_send, a_recv,
-    st_send, st_recv, h_send, h_recv, s_send, s_recv, o_sem, t_sem, small_sem,
+    st_send, st_recv, h_send, h_recv, s_send, s_recv, o_sem, t_sem, small_sem, met_sem, go_sem,
 ):
     sp, tp = lax.axis_index("sp"), lax.axis_index("tp")
     peer = 1 - tp
@@ -132,14 +132,25 @@
                 copy.start()
 
     barrier = pltpu.get_barrier_semaphore()
-    pl.semaphore_signal(barrier, inc=1, device_id={"tp": peer}, device_id_type=pl.DeviceIdType.MESH)
-    for step in range(1, n_sp):
-        pl.semaphore_signal(
-            barrier, inc=1, device_id={"sp": lax.rem(sp + step, n_sp)},
-            device_id_type=pl.DeviceIdType.MESH)
+
+    @pl.when(tp > 0)
+    def _():
+        pl.semaphore_wait(barrier, 1)
+        pl.semaphore_signal(met_sem, inc=1, device_id={"tp": peer}, device_id_type=pl.DeviceIdType.MESH)
+
+    @pl.when(tp == 0)
+    def _():
+        pl.semaphore_signal(barrier, inc=1, device_id={"tp": peer}, device_id_type=pl.DeviceIdType.MESH)
+        pl.semaphore_wait(met_sem, 1)
+
+        def greet(k, _):
+            pl.semaphore_signal(barrier, inc=1, device_id={"sp": k}, device_id_type=pl.DeviceIdType.MESH)
+            return 0
+
+        lax.fori_loop(0, sp, greet, 0)
+
     p_buf[pl.ds(0, BLOCK_ROWS), :] = jnp.zeros((BLOCK_ROWS, pool_w), BF16)
     state[...] = jnp.zeros_like(state)
-    pl.semaphore_wait(barrier, n_sp)
 
     for c in range(chunks):
         x_in(c).wait()
@@ -222,6 +233,15 @@
 
     second(chunks - 1, 0)
 
+    @pl.when((tp == 0) & (sp + 1 < n_sp))
+    def _():
+        pl.semaphore_wait(barrier, n_sp - 1 - sp)
+        pl.semaphore_signal(go_sem, inc=1, device_id={"tp": peer}, device_id_type=pl.DeviceIdType.MESH)
+
+    @pl.when((tp > 0) & (sp + 1 < n_sp))
+    def _():
+        pl.semaphore_wait(go_sem, 1)
+
     @pl.when(sp + 1 < n_sp)
     def _():
         h_out(sp + 1).start()
@@ -464,7 +484,7 @@
             dma((chunks,)), dma((chunks,)), dma((chunks,)), dma((5, n_tp)),
             dma((2,)), dma((2,)), dma((2,)), dma((2, chunks)), dma((2, chunks)),
             dma((n_sp,)), dma((n_sp,)), dma, dma, dma((chunks,)), dma((chunks,)), dma((chunks,)),
-            dma((chunks,)), dma((5,)),
+            dma((chunks,)), dma((5,)), pltpu.SemaphoreType.REGULAR, pltpu.SemaphoreType.REGULAR,
         ]
         row = lambda x: x.reshape(1, -1)
         resid, stats = pl.pallas_call(

time: 42.8 us -> 39.6 us (0.925)
  Pallas kernels: 42.7 us -> 39.5 us
    pallas_call x1, Pallas kernels: 38.8 us -> 35.6 us  [local(): pl.pallas_call(functools.partial(mixer, n_sp, n_tp, rows_x), out_shape=(j...]
where the time goes in v1:
time: 39.6 us; the launch traced here: 39.5 us
  Pallas kernels  39.5 us (100%)
    pallas_call x1, Pallas kernels, local(): pl.pallas_call(functools.partial(mixer, n_sp, n_tp, rows_x), out_shape=(j...  35.6 us
    pallas_call x1, Pallas kernels, local(): pl.pallas_call(functools.partial(finish, n_tp * feats, piece), out_shape=...  3.84 us

profile of v1, /device:TPU:0, one launch (start us, length us, event | category | flops | bytes accessed | tf_op | source)
XLA Modules:
  0.0 39.5 jit_solution(709982705412051038)
XLA Ops:
  0.0 35.6 %mixer.1 = (bf16[1024,1024]{1,0:T(8,128)(2,1)}, f32[1024,128]{1,0:T(8,128)}) custom-call(bf16[1,1024,1024]{2,1,0:T(8,128)(2,1)} %stream.1, bf16[2048,512]{1,0:T(8,128)(2,1)} %w_pool.1, bf16[2048,512]{1,0:T(8,128)(2,1)} %w_query.1, bf16[2048,512]{1,0:T(8,128)(2,1)} %w_forget.1, bf16[2048,512]{1,0:T(8,128)(2,1)} %w_value.1, bf16[2048,512]{1,0:T(8,128)(2,1)} %w_gate.1, ...), custom_call_target="tpu_custom_call" | custom-call | tf_op jit(solution)/shard_map/mixer/pallas_call | solution.py:490
  35.6 3.8 %finish.1 = bf16[1,1024,1024]{2,1,0:T(8,128)(2,1)} custom-call(bf16[1024,1024]{1,0:T(8,128)(2,1)} %get-tuple-element.7.resid, f32[1024,128]{1,0:T(8,128)} %get-tuple-element.8.stats, f32[1,1024]{1,0:T(1,128)} %bitcast.7, f32[1,1024]{1,0:T(1,128)} %bitcast.8), custom_call_target="tpu_custom_call" | custom-call | tf_op jit(solution)/shard_map/finish/pallas_call | solution.py:504

commit v2 on v0

v2 whole, which is shorter than its diff:
```python
import functools

import jax
import jax.numpy as jnp
from jax import lax
from jax.experimental import pallas as pl
from jax.experimental.pallas import tpu as pltpu
from jax.sharding import PartitionSpec as P

DK = 128
BLOCK_ROWS = 128
GROUP_CH = 256
HALO = 16
LANES = 128
ROWS = 256

ALPHA = 2.0**0.25
EPS_RMS = 1e-06
EPS_NORM = 1e-05
F32 = jnp.float32
BF16 = jnp.bfloat16
NT = (((1,), (1,)), ((), ()))
TN = (((0,), (0,)), ((), ()))
MESH = pl.DeviceIdType.MESH


def dot(a, b, dims=None):
    if dims is None:
        return jnp.dot(a, b, preferred_element_type=F32)
    return lax.dot_general(a, b, dims, preferred_element_type=F32)


def half_sigmoid(x):
    return 0.5 + 0.5 * jnp.tanh(0.5 * x)


def skew(items, stages, lag=1):
    items, count = list(items), 0
    order = []
    for t in range(len(items) + lag * (stages - 1)):
        for stage in reversed(range(stages)):
            if 0 <= t - stage * lag < len(items):
                order.append(t - stage * lag)
                count += 1

    def run():
        for i in order:
            next(items[i], None)
            yield

    return count, run()


def weave(bigs, smalls):
    n_big, n_small = (sum(n for n, _ in steps) for steps in (bigs, smalls))
    rest = [step for _, steps in smalls for step in [steps]]
    small = (None for steps in rest for _ in steps)
    done = 0
    for i, _ in enumerate(piece for _, steps in bigs for piece in steps):
        want = -(-(i + 1) * n_small // n_big)
        while done < want:
            next(small, None)
            done += 1
    for _ in small:
        pass


def mixer(
    n_sp, n_tp,
    stream, w_pool, w_query, w_forget, w_value, w_gate,
    mix_in, scale_in, bound_in, extra_in, gain_in, wo_pool, wo_rec, norm_gain_in, norm_bias_in,
    out,
    x_own, x_peer, w_buf, wo_own, wo_peer, a_own, a_peer, f_buf, v_buf, u_buf, e_buf, t_buf, p_buf, q_buf, sq_buf, g_buf, r_buf,
    o_buf, half_buf, state, state_out, state_in, halo_in, stat_own, stat_peer, norm_gain, norm_bias,
    mix, scale, bound, extra, extra_t, gain,
    x_loc, x_send, x_recv, w_sem, wo_loc, wo_send, wo_recv, a_send, a_recv,
    st_send, st_recv, h_send, h_recv, s_send, s_recv, o_sem, small_sem, met_sem, go_sem,
):
    sp, tp = lax.axis_index("sp"), lax.axis_index("tp")
    peer = 1 - tp
    length, feats = stream.shape[1], stream.shape[2]
    chans = bound.shape[1]
    heads = chans // DK
    pool_w = scale.shape[1]
    groups = mix.shape[0]
    chunks = length // ROWS
    blocks = length // BLOCK_ROWS
    per = ROWS // BLOCK_ROWS
    pair = 2 * DK

    def rows_of(c, size=ROWS, base=0):
        start = c * size + base
        return pl.ds(start if isinstance(start, int) else pl.multiple_of(start, BLOCK_ROWS), size)

    def x_in(c):
        rows = rows_of(c)
        return pltpu.make_async_copy(stream.at[0, rows], x_own.at[rows], x_loc.at[c])

    def x_out(c):
        rows = rows_of(c)
        return pltpu.make_async_remote_copy(
            x_own.at[rows], x_peer.at[rows], x_send.at[c], x_recv.at[c],
            device_id={"tp": peer}, device_id_type=MESH)

    def w_in(i, k):
        src = (w_forget, w_value, w_pool, w_query, w_gate)[i]
        rows = pl.ds(pl.multiple_of((tp, peer)[k] * feats, LANES), feats)
        return pltpu.make_async_copy(src.at[rows], w_buf.at[i, k], w_sem.at[i, k])

    my_cols = pl.ds(pl.multiple_of(tp * feats, LANES), feats)
    peer_cols = pl.ds(pl.multiple_of(peer * feats, LANES), feats)
    wo_places = ((wo_pool, pl.ds(0, pool_w)), (wo_rec, pl.ds(pool_w, chans)))

    def wo_in(i):
        src, place = wo_places[i]
        return pltpu.make_async_copy(src.at[:, my_cols], wo_own.at[place], wo_loc.at[i])

    def wo_out(i):
        src, place = wo_places[i]
        return pltpu.make_async_remote_copy(
            src.at[:, peer_cols], wo_peer.at[place], wo_send.at[i], wo_recv.at[i],
            device_id={"tp": peer}, device_id_type=MESH)

    def a_out(i, c):
        rows, cols = rows_of(c), wo_places[i][1]
        return pltpu.make_async_remote_copy(
            a_own.at[rows, cols], a_peer.at[rows, cols], a_send.at[i, c], a_recv.at[i, c],
            device_id={"tp": peer}, device_id_type=MESH)

    def st_out(pr):
        return pltpu.make_async_remote_copy(
            state_out.at[pr], state_in.at[pr], st_send.at[pr], st_recv.at[pr],
            device_id={"sp": lax.rem(sp + 1, n_sp)}, device_id_type=MESH)

    def h_out(k):
        return pltpu.make_async_remote_copy(
            p_buf.at[pl.ds(BLOCK_ROWS + length - HALO, HALO)], halo_in, h_send, h_recv,
            device_id={"sp": k}, device_id_type=MESH)

    def s_out(c):
        return pltpu.make_async_remote_copy(
            stat_own.at[c], stat_peer.at[c], s_send.at[c], s_recv.at[c],
            device_id={"tp": peer}, device_id_type=MESH)

    def o_out(c):
        rows = rows_of(c)
        return pltpu.make_async_copy(o_buf.at[rows], out.at[rows], o_sem.at[c])

    smalls = [
        pltpu.make_async_copy(src, dst, small_sem.at[i])
        for i, (src, dst) in enumerate(
            ((bound_in, bound), (extra_in, extra), (mix_in, mix), (scale_in, scale), (gain_in, gain),
             (norm_gain_in, norm_gain), (norm_bias_in, norm_bias)))
    ]

    barrier = pltpu.get_barrier_semaphore()

    @pl.when(tp == 0)
    def _():
        pl.semaphore_signal(barrier, inc=1, device_id={"tp": peer}, device_id_type=MESH)

    x_in(0).start()
    w_in(0, 0).start()
    for c in range(1, chunks):
        x_in(c).start()
    w_in(1, 0).start()
    for copy in smalls:
        copy.start()

    @pl.when(tp > 0)
    def _():
        pl.semaphore_wait(barrier, 1)
        pl.semaphore_signal(met_sem, inc=1, device_id={"tp": peer}, device_id_type=MESH)

    @pl.when(tp == 0)
    def _():
        pl.semaphore_wait(met_sem, 1)

    @pl.when((tp == 0) & (sp > 0))
    def _():
        pl.semaphore_signal(barrier, inc=1, device_id={"sp": lax.rem(sp + n_sp - 1, n_sp)}, device_id_type=MESH)

    p_buf[pl.ds(0, BLOCK_ROWS), :] = jnp.zeros((BLOCK_ROWS, pool_w), BF16)
    state[...] = jnp.zeros_like(state)

    row_ids = lax.broadcasted_iota(jnp.int32, (BLOCK_ROWS, BLOCK_ROWS), 0)
    col_ids = lax.broadcasted_iota(jnp.int32, (BLOCK_ROWS, BLOCK_ROWS), 1)
    lower = row_ids >= col_ids
    tri = jnp.where(lower, 1.0, 0.0).astype(BF16)
    tri_twice = jnp.concatenate([tri, tri], axis=1)

    def own_fv(c, i):
        rows = rows_of(c)
        r_buf[rows, i * chans:(i + 1) * chans] = dot(x_own[rows], w_buf[i, 0])

    def peer_fv(c, pr):
        rows = rows_of(c)
        cols = slice(pr * pair, (pr + 1) * pair)
        parts = [dot(x_peer[rows], w_buf[i, 1, :, cols]) for i in range(2)]
        for i, buf in ((0, f_buf), (1, v_buf)):
            both = slice(i * chans + pr * pair, i * chans + (pr + 1) * pair)
            buf[rows, cols] = (r_buf[rows, both] + parts[i]).astype(BF16)
        yield

    def project(c, i, buf, base=0):
        rows = rows_of(c)
        part = dot(x_own[rows], w_buf[i, 0])
        yield
        buf[rows_of(c, ROWS, base), :] = (part + dot(x_peer[rows], w_buf[i, 1])).astype(BF16)
        yield

    def gate_one(b, pr):
        brows = rows_of(b, BLOCK_ROWS)
        lanes = slice(pr * pair, (pr + 1) * pair)
        tile = BLOCK_ROWS // 4
        tiles = [slice(b * BLOCK_ROWS + k * tile, b * BLOCK_ROWS + (k + 1) * tile) for k in range(4)]
        weights, highs, lows = [], [], []
        for part in tiles:
            f_in = f_buf[part, lanes].astype(F32)
            drop = jnp.concatenate(
                [jnp.broadcast_to(extra_t[part, h:h + 1], (tile, DK)) for h in (2 * pr, 2 * pr + 1)], axis=1)
            weight = (1.0 - bound[:, lanes]) * (0.5 - 0.5 * jnp.tanh(0.5 * f_in))
            keep = jnp.log(1.0 - weight) + drop
            high = keep.astype(BF16)
            highs.append(high)
            lows.append((keep - high.astype(F32)).astype(BF16))
            e_buf[part, lanes] = weight
        total = dot(tri_twice, jnp.concatenate(highs + lows, axis=0))
        yield
        middle = 0.5 * total[BLOCK_ROWS - 1:BLOCK_ROWS]
        half = jnp.exp(middle)
        half_buf[b, :, lanes] = jnp.broadcast_to(half, (8, pair))
        downs = []
        for k, part in enumerate(tiles):
            apart = total[k * tile:(k + 1) * tile] - middle
            down = (e_buf[part, lanes] * jnp.exp(-apart)).astype(BF16)
            downs.append(down)
            u_buf[part, lanes] = down
            e_buf[part, lanes] = jnp.exp(apart)
        down = jnp.concatenate(downs, axis=0)
        terms = [
            dot(v_buf[brows, pr * pair + j * DK:pr * pair + (j + 1) * DK], down[:, j * DK:(j + 1) * DK], TN)
            for j in range(2)]
        yield
        term = jnp.concatenate(terms, axis=1) * half
        t_buf[b, :, lanes] = term
        state[:, lanes] = half * half * state[:, lanes] + term
        yield

    def gates(c, pr):
        return skew([gate_one(c * per + k, pr) for k in range(per)], 3)

    back = (lax.broadcasted_iota(jnp.int32, (BLOCK_ROWS, 2 * BLOCK_ROWS), 0) + BLOCK_ROWS
            - lax.broadcasted_iota(jnp.int32, (BLOCK_ROWS, 2 * BLOCK_ROWS), 1))
    count = lax.broadcasted_iota(jnp.int32, (BLOCK_ROWS, LANES), 0) + (sp * length + 1)

    def pool_one(b, j):
        start = b * BLOCK_ROWS
        brows = rows_of(b, BLOCK_ROWS)
        lanes = slice(j * GROUP_CH, (j + 1) * GROUP_CH)
        near = p_buf[rows_of(b, BLOCK_ROWS, 0), lanes]
        here = p_buf[rows_of(b, BLOCK_ROWS, BLOCK_ROWS), lanes]
        window = jnp.left_shift(jnp.int32(2), tp * groups + j)
        band = jnp.where((back >= 0) & (back < window), 1.0, 0.0).astype(BF16)
        sums = dot(band, jnp.concatenate([near, here], axis=0))
        yield
        share = 1.0 / jnp.minimum(count + start, window).astype(F32)
        share = jnp.concatenate([share] * (GROUP_CH // LANES), axis=1)
        diff = (sums * share - here.astype(F32)).astype(BF16)
        mixed = dot(diff, mix[j])
        yield
        a_own[brows, lanes] = (mixed * scale[:, lanes]).astype(BF16)
        yield

    def pools(c):
        return skew([pool_one(c * per + k, j) for k in range(per) for j in range(groups)], 3)

    def score_one(b, h):
        brows = rows_of(b, BLOCK_ROWS)
        lanes = slice(h * DK, (h + 1) * DK)
        q_in = q_buf[brows, lanes].astype(F32)
        up = (q_in * half_sigmoid(q_in) * e_buf[brows, lanes]).astype(BF16)
        sq_buf[brows, h * pair + DK:(h + 1) * pair] = up
        tile = dot(up, u_buf[brows, lanes], NT)
        yield
        sq_buf[brows, h * pair:h * pair + DK] = jnp.where(lower, tile, 0.0).astype(BF16)
        yield

    def scores(c):
        return skew([score_one(c * per + k, h) for k in range(per) for h in range(heads)], 2, 2)

    def mix_one(b, h):
        brows = rows_of(b, BLOCK_ROWS)
        lanes = slice(h * DK, (h + 1) * DK)
        half = half_buf[b, 0:1, lanes]
        before = state[:, lanes] * half
        state[:, lanes] = before * half + t_buf[b, :, lanes]
        carried = jnp.transpose(before.astype(BF16))
        yield
        raw = dot(sq_buf[brows, h * pair:(h + 1) * pair],
                  jnp.concatenate([v_buf[brows, lanes], carried], axis=0))
        yield
        power = jnp.mean(raw * raw, axis=-1, keepdims=True)
        yield
        gate = g_buf[brows, lanes].astype(F32)
        rec = raw * lax.rsqrt(power + EPS_RMS) * gain[...] * (gate * half_sigmoid(gate))
        a_own[brows, pool_w + h * DK:pool_w + (h + 1) * DK] = rec.astype(BF16)
        yield

    def mixes(c):
        return skew([mix_one(c * per + k, h) for k in range(per) for h in range(heads)], 4)

    with jax.named_scope("own_fv"):
        for c in range(chunks):
            if c < 2:
                for d in range(1) if c == 0 else range(1, chunks):
                    x_in(d).wait()
                    x_out(d).start()
            if c == 0:
                w_in(0, 0).wait()
                for i in range(2):
                    w_in(i, 1).start()
            own_fv(c, 0)
        w_in(1, 0).wait()
        for copy in smalls:
            copy.wait()
        for b in range(blocks):
            brows = rows_of(b, BLOCK_ROWS)
            extra_t[brows, 0:heads] = jnp.transpose(extra[:, brows])
        for c in range(chunks):
            own_fv(c, 1)

    for i in (2, 3, 4):
        for k in range(n_tp):
            w_in(i, k).start()
    for i in range(2):
        wo_in(i).start()
        wo_out(i).start()

    more = sp + 1 < n_sp

    def own_state(pr):
        @pl.when((sp == 0) & more)
        def _():
            state_out[pr] = state[:, pr * pair:(pr + 1) * pair].astype(BF16)
            st_out(pr).start()

    def next_state(pr, here):
        @pl.when(here & (sp > 0) & more)
        def _():
            lanes = slice(pr * pair, (pr + 1) * pair)
            root = half_buf[0, 0:1, lanes]
            for b in range(1, blocks):
                root = root * half_buf[b, 0:1, lanes]
            st_out(pr).wait_recv()
            state_out[pr] = (root * root * state_in[pr].astype(F32) + state[:, lanes]).astype(BF16)
            st_out(pr).start()

    fv_steps = [(c, pr) for pr in range(heads // 2) for c in range(chunks)]
    gate_items = [gate_one(b, pr) for pr in range(heads // 2) for b in range(blocks)]

    def fv_step(k):
        if k >= len(fv_steps):
            for _ in project(chunks - 1, 2, p_buf, BLOCK_ROWS):
                pass
            return
        c, pr = fv_steps[k]
        if pr == 0 and c % 2 == 0:
            for d in (c, c + 1):
                x_out(d).wait_recv()
        for _ in peer_fv(c, pr):
            pass

    def gate_slot(t):
        for stage in (2, 1, 0):
            if 0 <= t - stage < len(gate_items):
                next(gate_items[t - stage], None)

    for i in range(2):
        w_in(i, 1).wait()
    with jax.named_scope("fv"):
        fv_step(0)
        fv_step(1)
        for t in range(blocks + 2):
            if t % per == 0:
                fv_step(2 + t // per)
            gate_slot(t)

    with jax.named_scope("greet_wait"):
        @pl.when((tp == 0) & more)
        def _():
            pl.semaphore_wait(barrier, 1)
            pl.semaphore_signal(go_sem, inc=1, device_id={"tp": peer}, device_id_type=MESH)

        @pl.when((tp > 0) & more)
        def _():
            pl.semaphore_wait(go_sem, 1)

        own_state(0)

    for k in range(n_tp):
        w_in(2, k).wait()

    with jax.named_scope("fv_next"):
        for t in range(blocks + 2, 2 * blocks + 2):
            if t % per == 0 and 2 + t // per <= len(fv_steps):
                fv_step(2 + t // per)
            gate_slot(t)

    with jax.named_scope("sends"):
        @pl.when(more)
        def _():
            h_out(sp + 1).start()

        own_state(1)

    for i in (3, 4):
        for k in range(n_tp):
            w_in(i, k).wait()

    with jax.named_scope("pool_query"):
        for c in range(chunks - 1):
            weave([(2, project(c, 2, p_buf, BLOCK_ROWS))], [])
        next_state(0, sp == 1)
        weave([(2, project(0, 3, q_buf))], [])
        for c in range(1, chunks):
            weave([(2, project(c, 3, q_buf))], [scores(c - 1), pools(c)])
            if c == 1:
                next_state(1, sp == 1)
        for c in range(1, chunks):
            a_out(0, c).start()

    with jax.named_scope("halo_wait"):
        @pl.when(sp > 0)
        def _():
            h_out(sp).wait_recv()
            p_buf[pl.ds(BLOCK_ROWS - HALO, HALO), :] = halo_in[...]

        next_state(0, sp > 1)

    with jax.named_scope("gate0"):
        weave([(2, project(0, 4, g_buf))], [scores(chunks - 1), pools(0)])
        a_out(0, 0).start()
        next_state(1, sp > 1)

    with jax.named_scope("gate"):
        for c in range(1, chunks):
            weave([(2, project(c, 4, g_buf))], [])

    for i in range(2):
        wo_in(i).wait()
        wo_out(i).wait_recv()
    for c in range(chunks):
        a_out(0, c).wait_recv()
    pool_at, rec_at = (place for _, place in wo_places)

    def out_pool(c):
        rows = rows_of(c)
        for n in range(2):
            cols = slice(n * (feats // 2), (n + 1) * (feats // 2))
            r_buf[rows, cols] = (
                dot(a_own[rows, pool_at], wo_own[pool_at, cols])
                + dot(a_peer[rows, pool_at], wo_peer[pool_at, cols]))
            yield

    with jax.named_scope("out_pool0"):
        weave([(2, out_pool(0))], [])

    def first_state(pr):
        lanes = slice(pr * pair, (pr + 1) * pair)

        @pl.when((sp > 0) & (sp + 1 == n_sp))
        def _():
            st_out(pr).wait_recv()

        @pl.when(sp == 0)
        def _():
            state[:, lanes] = jnp.zeros((DK, pair), F32)

        @pl.when(sp > 0)
        def _():
            state[:, lanes] = state_in[pr].astype(F32)

    with jax.named_scope("join"):
        first_state(0)

    early = blocks // 2
    mix_items = [mix_one(b, h) for pr in range(heads // 2) for b in range(early) for h in (2 * pr, 2 * pr + 1)]
    mix_items += [mix_one(b, h) for b in range(early, blocks) for h in range(heads)]
    per_mix = per * heads

    def mix_slot(t):
        for stage in (3, 2, 1, 0):
            if 0 <= t - stage < len(mix_items):
                next(mix_items[t - stage], None)

    def fold(x):
        acc = x[:, :LANES]
        for k in range(1, x.shape[1] // LANES):
            acc = acc + x[:, k * LANES:(k + 1) * LANES]
        return acc

    first_half = lax.broadcasted_iota(jnp.int32, (32, LANES), 1) < LANES // 2

    def out_one(c, n):
        rows = rows_of(c)
        cols = slice(n * (feats // 2), (n + 1) * (feats // 2))
        full = (dot(a_own[rows, rec_at], wo_own[rec_at, cols])
                + dot(a_peer[rows, rec_at], wo_peer[rec_at, cols]))
        yield
        tile = 32
        for k in range(ROWS // tile):
            part = slice(c * ROWS + k * tile, c * ROWS + (k + 1) * tile)
            here = slice(k * tile, (k + 1) * tile)
            resid = full[here] + (r_buf[part, cols] + ALPHA * x_own[part, cols].astype(F32))
            r_buf[part, cols] = resid
            sums, squares = fold(resid), fold(resid * resid)
            both = jnp.where(first_half, sums + pltpu.roll(sums, LANES // 2, 1),
                             squares + pltpu.roll(squares, LANES // 2, 1))
            stat_own[c, here] = both if n == 0 else stat_own[c, here] + both
        if n == 1:
            s_out(c).start()
        yield

    def norm(c):
        def one(k):
            here = slice(k * 32, (k + 1) * 32)
            both = stat_own[c, here] + stat_peer[c, here]
            mean = jnp.sum(jnp.where(first_half, both, 0.0), axis=1, keepdims=True) / (n_tp * feats)
            square = jnp.sum(jnp.where(first_half, 0.0, both), axis=1, keepdims=True) / (n_tp * feats)
            inv = lax.rsqrt(square - mean * mean + EPS_NORM)
            yield
            part = slice(c * ROWS + k * 32, c * ROWS + (k + 1) * 32)
            for n in range(2):
                cols = slice(n * (feats // 2), (n + 1) * (feats // 2))
                o_buf[part, cols] = (
                    (r_buf[part, cols] - mean) * inv * norm_gain[:, cols] + norm_bias[:, cols]).astype(BF16)
            yield

        for _ in skew([one(k) for k in range(ROWS // 32)], 2, 3)[1]:
            pass
        o_out(c).start()

    with jax.named_scope("out_pool"):
        for c in range(1, chunks):
            weave([(2, out_pool(c))], [(per_mix, (mix_slot((c - 1) * per_mix + t) or t for t in range(per_mix)))])
            if c < heads // 2:
                first_state(c)
        for c in range(early // per):
            a_out(1, c).start()

    out_items = [out_one(c, n) for c in range(chunks) for n in range(2)]

    def out_slot(k):
        for stage in (1, 0):
            if 0 <= k - stage < len(out_items):
                next(out_items[k - stage], None)

    with jax.named_scope("out0"):
        for t in range(3):
            mix_slot((chunks - 1) * per_mix + t)
        for c in range(early // per, chunks - 1):
            a_out(1, c).start()
        a_out(1, 0).wait_recv()
        out_slot(0)
        for t in range(3, 3 + per_mix // 2):
            mix_slot((chunks - 1) * per_mix + t)
        out_slot(1)
        for t in range(3 + per_mix // 2, 3 + per_mix):
            mix_slot((chunks - 1) * per_mix + t)
        a_out(1, chunks - 1).start()

    with jax.named_scope("out1"):
        for c in range(1, chunks - 1):
            a_out(1, c).wait_recv()
        for k in range(2, 2 * chunks - 2):
            out_slot(k)

    with jax.named_scope("out3"):
        a_out(1, chunks - 1).wait_recv()
        for c in range(chunks - 2):
            s_out(c).wait_recv()
        out_slot(2 * chunks - 2)
        for c in range(chunks - 3):
            norm(c)
        out_slot(2 * chunks - 1)
        norm(chunks - 3)
        out_slot(2 * chunks)

    with jax.named_scope("stats"):
        for c in range(chunks - 2, chunks):
            s_out(c).wait_recv()
            norm(c)

    with jax.named_scope("drain"):
        for c in range(chunks):
            x_out(c).wait_send()
            s_out(c).wait_send()
            o_out(c).wait()
            for i in range(2):
                a_out(i, c).wait_send()
        for i in range(2):
            wo_out(i).wait_send()

        @pl.when(more)
        def _():
            for pr in range(heads // 2):
                st_out(pr).wait_send()

        @pl.when(sp + 1 < n_sp)
        def _():
            h_out(sp + 1).wait_send()


def finish(pieces, normed, out, buf, in_sem, out_sem):
    rows = normed.shape[0] // pieces

    def copies(c):
        part = pl.ds(c * rows, rows)
        return (
            pltpu.make_async_copy(normed.at[part], buf.at[part], in_sem.at[c]),
            pltpu.make_async_copy(buf.at[part], out.at[0, part], out_sem.at[c]),
        )

    for c in range(pieces):
        copies(c)[0].start()
    for c in range(pieces):
        copies(c)[0].wait()
        copies(c)[1].start()
    for c in range(pieces):
        copies(c)[1].wait()


def solution(mesh):
    n_sp, n_tp = mesh.shape["sp"], mesh.shape["tp"]

    def local(stream, w_pool, w_query, w_forget, w_value, w_gate, mix, scale, bound, extra,
              gain, wo_pool, wo_rec, norm_gain, norm_bias):
        length, feats = stream.shape[1], stream.shape[2]
        chans, pool_w = bound.shape[0], scale.shape[0]
        blocks = length // BLOCK_ROWS
        chunks = length // ROWS
        pairs = chans // DK // 2
        hbm = pl.BlockSpec(memory_space=pl.ANY)
        dma = pltpu.SemaphoreType.DMA
        scratch = [
            pltpu.VMEM((length, feats), BF16),
            pltpu.VMEM((length, feats), BF16),
            pltpu.VMEM((5, n_tp, feats, chans), BF16),
            pltpu.VMEM((pool_w + chans, feats), BF16),
            pltpu.VMEM((pool_w + chans, feats), BF16),
            pltpu.VMEM((length, pool_w + chans), BF16),
            pltpu.VMEM((length, pool_w + chans), BF16),
            pltpu.VMEM((length, chans), BF16),
            pltpu.VMEM((length, chans), BF16),
            pltpu.VMEM((length, chans), BF16),
            pltpu.VMEM((length, chans), F32),
            pltpu.VMEM((blocks, DK, chans), F32),
            pltpu.VMEM((BLOCK_ROWS + length, pool_w), BF16),
            pltpu.VMEM((length, chans), BF16),
            pltpu.VMEM((length, 2 * chans), BF16),
            pltpu.VMEM((length, chans), BF16),
            pltpu.VMEM((length, max(feats, 2 * chans)), F32),
            pltpu.VMEM((length, feats), BF16),
            pltpu.VMEM((blocks, 8, chans), F32),
            pltpu.VMEM((DK, chans), F32),
            pltpu.VMEM((pairs, DK, 2 * DK), BF16),
            pltpu.VMEM((pairs, DK, 2 * DK), BF16),
            pltpu.VMEM((HALO, pool_w), BF16),
            pltpu.VMEM((chunks, ROWS, LANES), F32),
            pltpu.VMEM((chunks, ROWS, LANES), F32),
            pltpu.VMEM((1, feats), F32),
            pltpu.VMEM((1, feats), F32),
            pltpu.VMEM(mix.shape, BF16),
            pltpu.VMEM((1, pool_w), F32),
            pltpu.VMEM((1, chans), F32),
            pltpu.VMEM((chans // DK, length), F32),
            pltpu.VMEM((length, LANES), F32),
            pltpu.VMEM((1, DK), F32),
            dma((chunks,)), dma((chunks,)), dma((chunks,)), dma((5, n_tp)),
            dma((2,)), dma((2,)), dma((2,)), dma((2, chunks)), dma((2, chunks)),
            dma((pairs,)), dma((pairs,)), dma, dma, dma((chunks,)), dma((chunks,)), dma((chunks,)),
            dma((7,)), pltpu.SemaphoreType.REGULAR, pltpu.SemaphoreType.REGULAR,
        ]
        row = lambda x: x.reshape(1, -1)
        normed = pl.pallas_call(
            functools.partial(mixer, n_sp, n_tp),
            out_shape=jax.ShapeDtypeStruct((length, feats), BF16),
            in_specs=[hbm] * 15,
            out_specs=hbm,
            scratch_shapes=scratch,
            compiler_params=pltpu.CompilerParams(
                collective_id=0, has_side_effects=True, vmem_limit_bytes=60 * 1024 * 1024),
            name="mixer",
        )(stream, w_pool, w_query, w_forget, w_value, w_gate, mix, row(scale), row(bound), extra.T,
          row(gain), wo_pool, wo_rec, row(norm_gain), row(norm_bias))
        pieces = 8
        return pl.pallas_call(
            functools.partial(finish, pieces),
            out_shape=jax.ShapeDtypeStruct(stream.shape, BF16),
            in_specs=[hbm],
            out_specs=hbm,
            scratch_shapes=[pltpu.VMEM((length, feats), BF16), dma((pieces,)), dma((pieces,))],
            compiler_params=pltpu.CompilerParams(vmem_limit_bytes=60 * 1024 * 1024),
            name="finish",
        )(normed)

    placed = (
        P("fs", "sp", "tp"), P(None, "tp"), P(None, "tp"), P(None, "tp"), P(None, "tp"),
        P(None, "tp"), P("tp", None, None), P("tp"), P("tp"), P("sp", "tp"), P(),
        P("tp", None), P("tp", None), P("tp"), P("tp"),
    )
    return jax.shard_map(
        local, mesh=mesh, in_specs=placed, out_specs=P("fs", "sp", "tp"), check_vma=False
    )
```

time: 42.8 us -> 34.4 us (0.80)
  Pallas kernels: 42.7 us -> 33.9 us
    pallas_call x2, Pallas kernels: 42.7 us -> 33.9 us  [the longest x1 31.5 us: local(): pl.pallas_call(functools.partial(mixer, n_sp, n_tp), out_shape=jax.ShapeD...]
where the time goes in v2:
time: 34.4 us; the launch traced here: 34.1 us
  Pallas kernels  33.9 us (99%)
    pallas_call x1, Pallas kernels, local(): pl.pallas_call(functools.partial(mixer, n_sp, n_tp), out_shape=jax.ShapeD...  31.5 us
    pallas_call x1, Pallas kernels, local(): pl.pallas_call(functools.partial(finish, pieces), out_shape=jax.ShapeDtyp...  2.39 us

profile of v2, /device:TPU:0, one launch (start us, length us, event | category | flops | bytes accessed | tf_op | source)
XLA Modules:
  0.0 34.1 jit_solution(14401850922445016113)
XLA Ops:
  0.0 31.5 %mixer.1.normed = bf16[1024,1024]{1,0:T(8,128)(2,1)} custom-call(bf16[1,1024,1024]{2,1,0:T(8,128)(2,1)} %stream.1, bf16[2048,512]{1,0:T(8,128)(2,1)} %w_pool.1, bf16[2048,512]{1,0:T(8,128)(2,1)} %w_query.1, bf16[2048,512]{1,0:T(8,128)(2,1)} %w_forget.1, bf16[2048,512]{1,0:T(8,128)(2,1)} %w_value.1, bf16[2048,512]{1,0:T(8,128)(2,1)} %w_gate.1, ...), custom_call_target="tpu_custom_call" | custom-call | tf_op jit(solution)/shard_map/mixer/pallas_call | solution.py:686
  31.5 2.4 %finish.1 = bf16[1,1024,1024]{2,1,0:T(8,128)(2,1)} custom-call(bf16[1024,1024]{1,0:T(8,128)(2,1)} %mixer.1.normed), custom_call_target="tpu_custom_call" | custom-call | tf_op jit(solution)/shard_map/finish/pallas_call | solution.py:698

commit v3 on v2

--- a/solution.py
+++ b/solution.py
@@ -70,10 +70,10 @@
     stream, w_pool, w_query, w_forget, w_value, w_gate,
     mix_in, scale_in, bound_in, extra_in, gain_in, wo_pool, wo_rec, norm_gain_in, norm_bias_in,
     out,
-    x_own, x_peer, w_buf, wo_own, wo_peer, a_own, a_peer, f_buf, v_buf, u_buf, e_buf, t_buf, p_buf, q_buf, sq_buf, g_buf, r_buf,
+    x_own, x_peer, w_buf, fv_buf, wo_own, wo_peer, a_own, a_peer, f_buf, v_buf, u_buf, e_buf, t_buf, p_buf, q_buf, sq_buf, g_buf, r_buf,
     o_buf, half_buf, state, state_out, state_in, halo_in, stat_own, stat_peer, norm_gain, norm_bias,
     mix, scale, bound, extra, extra_t, gain,
-    x_loc, x_send, x_recv, w_sem, wo_loc, wo_send, wo_recv, a_send, a_recv,
+    x_loc, x_send, x_recv, w_sem, fv_sem, wo_loc, wo_send, wo_recv, a_send, a_recv,
     st_send, st_recv, h_send, h_recv, s_send, s_recv, o_sem, small_sem, met_sem, go_sem,
 ):
     sp, tp = lax.axis_index("sp"), lax.axis_index("tp")
@@ -102,10 +102,19 @@
             x_own.at[rows], x_peer.at[rows], x_send.at[c], x_recv.at[c],
             device_id={"tp": peer}, device_id_type=MESH)
 
+    def w_rows(k):
+        return pl.ds(pl.multiple_of((tp, peer)[k] * feats, LANES), feats)
+
     def w_in(i, k):
-        src = (w_forget, w_value, w_pool, w_query, w_gate)[i]
-        rows = pl.ds(pl.multiple_of((tp, peer)[k] * feats, LANES), feats)
-        return pltpu.make_async_copy(src.at[rows], w_buf.at[i, k], w_sem.at[i, k])
+        src = (w_pool, w_query, w_gate)[i]
+        return pltpu.make_async_copy(src.at[w_rows(k)], w_buf.at[i, k], w_sem.at[i, k])
+
+    def fv_in(pr, k):
+        return [
+            pltpu.make_async_copy(
+                src.at[w_rows(k), pl.ds(pr * pair, pair)], fv_buf.at[pr, k, :, pl.ds(i * pair, pair)],
+                fv_sem.at[pr, k, i])
+            for i, src in enumerate((w_forget, w_value))]
 
     my_cols = pl.ds(pl.multiple_of(tp * feats, LANES), feats)
     peer_cols = pl.ds(pl.multiple_of(peer * feats, LANES), feats)
@@ -159,14 +168,10 @@
     def _():
         pl.semaphore_signal(barrier, inc=1, device_id={"tp": peer}, device_id_type=MESH)
 
+    n_pairs = heads // 2
     x_in(0).start()
-    w_in(0, 0).start()
-    for c in range(1, chunks):
-        x_in(c).start()
-    w_in(1, 0).start()
-    for copy in smalls:
+    for copy in fv_in(0, 0):
         copy.start()
-
     @pl.when(tp > 0)
     def _():
         pl.semaphore_wait(barrier, 1)
@@ -179,6 +184,14 @@
     @pl.when((tp == 0) & (sp > 0))
     def _():
         pl.semaphore_signal(barrier, inc=1, device_id={"sp": lax.rem(sp + n_sp - 1, n_sp)}, device_id_type=MESH)
+
+    for c in range(1, chunks):
+        x_in(c).start()
+    for pr in range(1, n_pairs):
+        for copy in fv_in(pr, 0):
+            copy.start()
+    for copy in smalls:
+        copy.start()
 
     p_buf[pl.ds(0, BLOCK_ROWS), :] = jnp.zeros((BLOCK_ROWS, pool_w), BF16)
     state[...] = jnp.zeros_like(state)
@@ -189,17 +202,17 @@
     tri = jnp.where(lower, 1.0, 0.0).astype(BF16)
     tri_twice = jnp.concatenate([tri, tri], axis=1)
 
-    def own_fv(c, i):
+    def own_fv(c, pr):
         rows = rows_of(c)
-        r_buf[rows, i * chans:(i + 1) * chans] = dot(x_own[rows], w_buf[i, 0])
+        r_buf[rows, 2 * pr * pair:2 * (pr + 1) * pair] = dot(x_own[rows], fv_buf[pr, 0])
 
     def peer_fv(c, pr):
         rows = rows_of(c)
         cols = slice(pr * pair, (pr + 1) * pair)
-        parts = [dot(x_peer[rows], w_buf[i, 1, :, cols]) for i in range(2)]
+        part = dot(x_peer[rows], fv_buf[pr, 1])
         for i, buf in ((0, f_buf), (1, v_buf)):
-            both = slice(i * chans + pr * pair, i * chans + (pr + 1) * pair)
-            buf[rows, cols] = (r_buf[rows, both] + parts[i]).astype(BF16)
+            base = (2 * pr + i) * pair
+            buf[rows, cols] = (r_buf[rows, base:base + pair] + part[:, i * pair:(i + 1) * pair]).astype(BF16)
         yield
 
     def project(c, i, buf, base=0):
@@ -311,26 +324,32 @@
         return skew([mix_one(c * per + k, h) for k in range(per) for h in range(heads)], 4)
 
     with jax.named_scope("own_fv"):
-        for c in range(chunks):
-            if c < 2:
-                for d in range(1) if c == 0 else range(1, chunks):
-                    x_in(d).wait()
-                    x_out(d).start()
-            if c == 0:
-                w_in(0, 0).wait()
-                for i in range(2):
-                    w_in(i, 1).start()
+        x_in(0).wait()
+        x_out(0).start()
+        for copy in fv_in(0, 0):
+            copy.wait()
+        own_fv(0, 0)
+        for c in range(1, chunks):
+            x_in(c).wait()
+            x_out(c).start()
+        for pr in range(n_pairs):
+            for copy in fv_in(pr, 1):
+                copy.start()
+        for c in range(1, chunks):
             own_fv(c, 0)
-        w_in(1, 0).wait()
+        for pr in range(1, n_pairs):
+            for copy in fv_in(pr, 0):
+                copy.wait()
         for copy in smalls:
             copy.wait()
         for b in range(blocks):
             brows = rows_of(b, BLOCK_ROWS)
             extra_t[brows, 0:heads] = jnp.transpose(extra[:, brows])
-        for c in range(chunks):
-            own_fv(c, 1)
-
-    for i in (2, 3, 4):
+        for pr in range(1, n_pairs):
+            for c in range(chunks):
+                own_fv(c, pr)
+
+    for i in range(3):
         for k in range(n_tp):
             w_in(i, k).start()
     for i in range(2):
@@ -361,7 +380,7 @@
 
     def fv_step(k):
         if k >= len(fv_steps):
-            for _ in project(chunks - 1, 2, p_buf, BLOCK_ROWS):
+            for _ in project(chunks - 1, 0, p_buf, BLOCK_ROWS):
                 pass
             return
         c, pr = fv_steps[k]
@@ -376,8 +395,9 @@
             if 0 <= t - stage < len(gate_items):
                 next(gate_items[t - stage], None)
 
-    for i in range(2):
-        w_in(i, 1).wait()
+    for pr in range(n_pairs):
+        for copy in fv_in(pr, 1):
+            copy.wait()
     with jax.named_scope("fv"):
         fv_step(0)
         fv_step(1)
@@ -399,7 +419,7 @@
         own_state(0)
 
     for k in range(n_tp):
-        w_in(2, k).wait()
+        w_in(0, k).wait()
 
     with jax.named_scope("fv_next"):
         for t in range(blocks + 2, 2 * blocks + 2):
@@ -414,17 +434,17 @@
 
         own_state(1)
 
-    for i in (3, 4):
+    for i in (1, 2):
         for k in range(n_tp):
             w_in(i, k).wait()
 
     with jax.named_scope("pool_query"):
         for c in range(chunks - 1):
-            weave([(2, project(c, 2, p_buf, BLOCK_ROWS))], [])
+            weave([(2, project(c, 0, p_buf, BLOCK_ROWS))], [])
         next_state(0, sp == 1)
-        weave([(2, project(0, 3, q_buf))], [])
+        weave([(2, project(0, 1, q_buf))], [])
         for c in range(1, chunks):
-            weave([(2, project(c, 3, q_buf))], [scores(c - 1), pools(c)])
+            weave([(2, project(c, 1, q_buf))], [scores(c - 1), pools(c)])
             if c == 1:
                 next_state(1, sp == 1)
         for c in range(1, chunks):
@@ -439,13 +459,13 @@
         next_state(0, sp > 1)
 
     with jax.named_scope("gate0"):
-        weave([(2, project(0, 4, g_buf))], [scores(chunks - 1), pools(0)])
+        weave([(2, project(0, 2, g_buf))], [scores(chunks - 1), pools(0)])
         a_out(0, 0).start()
         next_state(1, sp > 1)
 
     with jax.named_scope("gate"):
         for c in range(1, chunks):
-            weave([(2, project(c, 4, g_buf))], [])
+            weave([(2, project(c, 2, g_buf))], [])
 
     for i in range(2):
         wo_in(i).wait()
@@ -484,9 +504,9 @@
     with jax.named_scope("join"):
         first_state(0)
 
-    early = blocks // 2
-    mix_items = [mix_one(b, h) for pr in range(heads // 2) for b in range(early) for h in (2 * pr, 2 * pr + 1)]
-    mix_items += [mix_one(b, h) for b in range(early, blocks) for h in range(heads)]
+    mix_items = [
+        mix_one(c * per + k, h) for c in range(chunks) for pr in range(n_pairs) for k in range(per)
+        for h in (2 * pr, 2 * pr + 1)]
     per_mix = per * heads
 
     def mix_slot(t):
@@ -541,36 +561,42 @@
             pass
         o_out(c).start()
 
+    def mix_slots(first, last):
+        for t in range(first, min(last, len(mix_items) + 3)):
+            mix_slot(t)
+            if t % per_mix == 2 and t >= per_mix:
+                a_out(1, t // per_mix - 1).start()
+
+    pieces = [(c, n) for c in range(1, chunks) for n in range(2)]
+    per_piece = -(-(len(mix_items) + 3) // (len(pieces) + 1))
+
     with jax.named_scope("out_pool"):
-        for c in range(1, chunks):
-            weave([(2, out_pool(c))], [(per_mix, (mix_slot((c - 1) * per_mix + t) or t for t in range(per_mix)))])
-            if c < heads // 2:
-                first_state(c)
-        for c in range(early // per):
-            a_out(1, c).start()
+        for k, (c, n) in enumerate(pieces):
+            if n == 0:
+                step = out_pool(c)
+            next(step, None)
+            if k == 0:
+                mix_slots(0, per_mix // n_pairs)
+                for pr in range(1, n_pairs):
+                    first_state(pr)
+                mix_slots(per_mix // n_pairs, per_piece)
+            else:
+                mix_slots(k * per_piece, (k + 1) * per_piece)
 
     out_items = [out_one(c, n) for c in range(chunks) for n in range(2)]
 
     def out_slot(k):
-        for stage in (1, 0):
+        for stage in (0, 1):
             if 0 <= k - stage < len(out_items):
                 next(out_items[k - stage], None)
 
     with jax.named_scope("out0"):
-        for t in range(3):
-            mix_slot((chunks - 1) * per_mix + t)
-        for c in range(early // per, chunks - 1):
-            a_out(1, c).start()
         a_out(1, 0).wait_recv()
         out_slot(0)
-        for t in range(3, 3 + per_mix // 2):
-            mix_slot((chunks - 1) * per_mix + t)
+        mix_slots(len(pieces) * per_piece, len(mix_items) + 3)
         out_slot(1)
-        for t in range(3 + per_mix // 2, 3 + per_mix):
-            mix_slot((chunks - 1) * per_mix + t)
-        a_out(1, chunks - 1).start()
-
-    with jax.named_scope("out1"):
+
+    with jax.named_scope("out2"):
         for c in range(1, chunks - 1):
             a_out(1, c).wait_recv()
         for k in range(2, 2 * chunks - 2):
@@ -578,17 +604,15 @@
 
     with jax.named_scope("out3"):
         a_out(1, chunks - 1).wait_recv()
-        for c in range(chunks - 2):
+        out_slot(2 * chunks - 2)
+        out_slot(2 * chunks - 1)
+        for c in range(chunks - 3):
             s_out(c).wait_recv()
-        out_slot(2 * chunks - 2)
-        for c in range(chunks - 3):
             norm(c)
-        out_slot(2 * chunks - 1)
-        norm(chunks - 3)
         out_slot(2 * chunks)
 
     with jax.named_scope("stats"):
-        for c in range(chunks - 2, chunks):
+        for c in range(chunks - 3, chunks):
             s_out(c).wait_recv()
             norm(c)
 
@@ -646,7 +670,8 @@
         scratch = [
             pltpu.VMEM((length, feats), BF16),
             pltpu.VMEM((length, feats), BF16),
-            pltpu.VMEM((5, n_tp, feats, chans), BF16),
+            pltpu.VMEM((3, n_tp, feats, chans), BF16),
+            pltpu.VMEM((pairs, n_tp, feats, 4 * DK), BF16),
             pltpu.VMEM((pool_w + chans, feats), BF16),
             pltpu.VMEM((pool_w + chans, feats), BF16),
             pltpu.VMEM((length, pool_w + chans), BF16),
@@ -677,7 +702,7 @@
             pltpu.VMEM((chans // DK, length), F32),
             pltpu.VMEM((length, LANES), F32),
             pltpu.VMEM((1, DK), F32),
-            dma((chunks,)), dma((chunks,)), dma((chunks,)), dma((5, n_tp)),
+            dma((chunks,)), dma((chunks,)), dma((chunks,)), dma((3, n_tp)), dma((pairs, n_tp, 2)),
             dma((2,)), dma((2,)), dma((2,)), dma((2, chunks)), dma((2, chunks)),
             dma((pairs,)), dma((pairs,)), dma, dma, dma((chunks,)), dma((chunks,)), dma((chunks,)),
             dma((7,)), pltpu.SemaphoreType.REGULAR, pltpu.SemaphoreType.REGULAR,
@@ -694,7 +719,7 @@
             name="mixer",
         )(stream, w_pool, w_query, w_forget, w_value, w_gate, mix, row(scale), row(bound), extra.T,
           row(gain), wo_pool, wo_rec, row(norm_gain), row(norm_bias))
-        pieces = 8
+        pieces = 4
         return pl.pallas_call(
             functools.partial(finish, pieces),
             out_shape=jax.ShapeDtypeStruct(stream.shape, BF16),

time: 34.4 us -> 32.1 us (0.933)
  Pallas kernels: 33.9 us -> 31.3 us
    pallas_call x1, Pallas kernels: 31.5 us -> 28.9 us  [local(): pl.pallas_call(functools.partial(mixer, n_sp, n_tp), out_shape=jax.ShapeD...]
where the time goes in v3:
time: 32.1 us; the launch traced here: 31.5 us
  Pallas kernels  31.3 us (98%)
    pallas_call x1, Pallas kernels, local(): pl.pallas_call(functools.partial(mixer, n_sp, n_tp), out_shape=jax.ShapeD...  28.9 us
    pallas_call x1, Pallas kernels, local(): pl.pallas_call(functools.partial(finish, pieces), out_shape=jax.ShapeDtyp...  2.42 us

profile of v3, /device:TPU:0, one launch (start us, length us, event | category | flops | bytes accessed | tf_op | source)
XLA Modules:
  0.0 31.5 jit_solution(14744342976243144839)
XLA Ops:
  0.0 28.9 %mixer.1.normed = bf16[1024,1024]{1,0:T(8,128)(2,1)} custom-call(bf16[1,1024,1024]{2,1,0:T(8,128)(2,1)} %stream.1, bf16[2048,512]{1,0:T(8,128)(2,1)} %w_pool.1, bf16[2048,512]{1,0:T(8,128)(2,1)} %w_query.1, bf16[2048,512]{1,0:T(8,128)(2,1)} %w_forget.1, bf16[2048,512]{1,0:T(8,128)(2,1)} %w_value.1, bf16[2048,512]{1,0:T(8,128)(2,1)} %w_gate.1, ...), custom_call_target="tpu_custom_call" | custom-call | tf_op jit(solution)/shard_map/mixer/pallas_call | solution.py:711
  28.9 2.4 %finish.1 = bf16[1,1024,1024]{2,1,0:T(8,128)(2,1)} custom-call(bf16[1024,1024]{1,0:T(8,128)(2,1)} %mixer.1.normed), custom_call_target="tpu_custom_call" | custom-call | tf_op jit(solution)/shard_map/finish/pallas_call | solution.py:723

commit v4 on v3

--- a/solution.py
+++ b/solution.py
@@ -286,7 +286,7 @@
         yield
 
     def pools(c):
-        return skew([pool_one(c * per + k, j) for k in range(per) for j in range(groups)], 3)
+        return skew([pool_one(c * per + k, j) for k in range(per) for j in range(groups)], 3, 2)
 
     def score_one(b, h):
         brows = rows_of(b, BLOCK_ROWS)
@@ -300,7 +300,7 @@
         yield
 
     def scores(c):
-        return skew([score_one(c * per + k, h) for k in range(per) for h in range(heads)], 2, 2)
+        return skew([score_one(c * per + k, h) for k in range(per) for h in range(heads)], 2, 3)
 
     def mix_one(b, h):
         brows = rows_of(b, BLOCK_ROWS)
@@ -390,10 +390,12 @@
         for _ in peer_fv(c, pr):
             pass
 
+    gate_lag = 2
+
     def gate_slot(t):
         for stage in (2, 1, 0):
-            if 0 <= t - stage < len(gate_items):
-                next(gate_items[t - stage], None)
+            if 0 <= t - gate_lag * stage < len(gate_items):
+                next(gate_items[t - gate_lag * stage], None)
 
     for pr in range(n_pairs):
         for copy in fv_in(pr, 1):
@@ -401,7 +403,7 @@
     with jax.named_scope("fv"):
         fv_step(0)
         fv_step(1)
-        for t in range(blocks + 2):
+        for t in range(blocks + 2 * gate_lag):
             if t % per == 0:
                 fv_step(2 + t // per)
             gate_slot(t)
@@ -422,7 +424,7 @@
         w_in(0, k).wait()
 
     with jax.named_scope("fv_next"):
-        for t in range(blocks + 2, 2 * blocks + 2):
+        for t in range(blocks + 2 * gate_lag, 2 * blocks + 2 * gate_lag):
             if t % per == 0 and 2 + t // per <= len(fv_steps):
                 fv_step(2 + t // per)
             gate_slot(t)
@@ -509,10 +511,12 @@
         for h in (2 * pr, 2 * pr + 1)]
     per_mix = per * heads
 
+    mix_lags = (0, 2, 4, 5)
+
     def mix_slot(t):
         for stage in (3, 2, 1, 0):
-            if 0 <= t - stage < len(mix_items):
-                next(mix_items[t - stage], None)
+            if 0 <= t - mix_lags[stage] < len(mix_items):
+                next(mix_items[t - mix_lags[stage]], None)
 
     def fold(x):
         acc = x[:, :LANES]
@@ -562,13 +566,13 @@
         o_out(c).start()
 
     def mix_slots(first, last):
-        for t in range(first, min(last, len(mix_items) + 3)):
+        for t in range(first, min(last, len(mix_items) + mix_lags[3])):
             mix_slot(t)
-            if t % per_mix == 2 and t >= per_mix:
+            if t % per_mix == mix_lags[3] - 1 and t >= per_mix:
                 a_out(1, t // per_mix - 1).start()
 
     pieces = [(c, n) for c in range(1, chunks) for n in range(2)]
-    per_piece = -(-(len(mix_items) + 3) // (len(pieces) + 1))
+    per_piece = -(-(len(mix_items) + mix_lags[3]) // (len(pieces) + 1))
 
     with jax.named_scope("out_pool"):
         for k, (c, n) in enumerate(pieces):
@@ -593,7 +597,7 @@
     with jax.named_scope("out0"):
         a_out(1, 0).wait_recv()
         out_slot(0)
-        mix_slots(len(pieces) * per_piece, len(mix_items) + 3)
+        mix_slots(len(pieces) * per_piece, len(mix_items) + mix_lags[3])
         out_slot(1)
 
     with jax.named_scope("out2"):

time: 32.1 us -> 31.1 us (0.969)
  the two profiles are of different devices: /device:TPU:0 before, /device:TPU:15 now
where the time goes in v4:
time: 31.1 us; the launch traced here: 31 us
  Pallas kernels  30.8 us (99%)
    pallas_call x1, Pallas kernels, local(): pl.pallas_call(functools.partial(mixer, n_sp, n_tp), out_shape=jax.ShapeD...  28.4 us
    pallas_call x1, Pallas kernels, local(): pl.pallas_call(functools.partial(finish, pieces), out_shape=jax.ShapeDtyp...  2.42 us

profile of v4, /device:TPU:15, one launch (start us, length us, event | category | flops | bytes accessed | tf_op | source)
XLA Modules:
  0.0 31.0 jit_solution(12142805541812147252)
XLA Ops:
  0.0 28.4 %mixer.1.normed = bf16[1024,1024]{1,0:T(8,128)(2,1)} custom-call(bf16[1,1024,1024]{2,1,0:T(8,128)(2,1)} %stream.1, bf16[2048,512]{1,0:T(8,128)(2,1)} %w_pool.1, bf16[2048,512]{1,0:T(8,128)(2,1)} %w_query.1, bf16[2048,512]{1,0:T(8,128)(2,1)} %w_forget.1, bf16[2048,512]{1,0:T(8,128)(2,1)} %w_value.1, bf16[2048,512]{1,0:T(8,128)(2,1)} %w_gate.1, ...), custom_call_target="tpu_custom_call" | custom-call | tf_op jit(solution)/shard_map/mixer/pallas_call | solution.py:715
  28.4 2.4 %finish.1 = bf16[1,1024,1024]{2,1,0:T(8,128)(2,1)} custom-call(bf16[1024,1024]{1,0:T(8,128)(2,1)} %mixer.1.normed), custom_call_target="tpu_custom_call" | custom-call | tf_op jit(solution)/shard_map/finish/pallas_call | solution.py:727

commit v5 on v4

--- a/solution.py
+++ b/solution.py
@@ -393,7 +393,7 @@
     gate_lag = 2
 
     def gate_slot(t):
-        for stage in (2, 1, 0):
+        for stage in (0, 2, 1):
             if 0 <= t - gate_lag * stage < len(gate_items):
                 next(gate_items[t - gate_lag * stage], None)
 
@@ -511,7 +511,7 @@
         for h in (2 * pr, 2 * pr + 1)]
     per_mix = per * heads
 
-    mix_lags = (0, 2, 4, 5)
+    mix_lags = (0, 2, 5, 7)
 
     def mix_slot(t):
         for stage in (3, 2, 1, 0):
@@ -610,10 +610,10 @@
         a_out(1, chunks - 1).wait_recv()
         out_slot(2 * chunks - 2)
         out_slot(2 * chunks - 1)
+        out_slot(2 * chunks)
         for c in range(chunks - 3):
             s_out(c).wait_recv()
             norm(c)
-        out_slot(2 * chunks)
 
     with jax.named_scope("stats"):
         for c in range(chunks - 3, chunks):

time: 31.1 us -> 30.7 us (0.987)
  the two profiles are of different devices: /device:TPU:15 before, /device:TPU:0 now
where the time goes in v5:
time: 30.7 us; the launch traced here: 30 us
  Pallas kernels  29.9 us (97%)
    pallas_call x1, Pallas kernels, local(): pl.pallas_call(functools.partial(mixer, n_sp, n_tp), out_shape=jax.ShapeD...  27.5 us
    pallas_call x1, Pallas kernels, local(): pl.pallas_call(functools.partial(finish, pieces), out_shape=jax.ShapeDtyp...  2.42 us

profile of v5, /device:TPU:0, one launch (start us, length us, event | category | flops | bytes accessed | tf_op | source)
XLA Modules:
  0.0 30.0 jit_solution(2563866661170960483)
XLA Ops:
  0.0 27.5 %mixer.1.normed = bf16[1024,1024]{1,0:T(8,128)(2,1)} custom-call(bf16[1,1024,1024]{2,1,0:T(8,128)(2,1)} %stream.1, bf16[2048,512]{1,0:T(8,128)(2,1)} %w_pool.1, bf16[2048,512]{1,0:T(8,128)(2,1)} %w_query.1, bf16[2048,512]{1,0:T(8,128)(2,1)} %w_forget.1, bf16[2048,512]{1,0:T(8,128)(2,1)} %w_value.1, bf16[2048,512]{1,0:T(8,128)(2,1)} %w_gate.1, ...), custom_call_target="tpu_custom_call" | custom-call | tf_op jit(solution)/shard_map/mixer/pallas_call | solution.py:715
  27.5 2.4 %finish.1 = bf16[1,1024,1024]{2,1,0:T(8,128)(2,1)} custom-call(bf16[1024,1024]{1,0:T(8,128)(2,1)} %mixer.1.normed), custom_call_target="tpu_custom_call" | custom-call | tf_op jit(solution)/shard_map/finish/pallas_call | solution.py:727
